TPU v7x, 256 devices: a whole 4x4x8 slice. The times are simulated.
256 devices in a mesh: ep: 128 (over z, y, x), tp: 2 (over core).
Axes of the slice: x: 4, y: 4, z: 8, core: 2. Of those that a mesh axis runs over, the one named last changes fastest.
Arguments:
- tokens: bfloat16 [65536, 2048], P(('ep', 'tp')), may hold values from -6 to 6
- norm_gain: float32 [2048], replicated, may hold values from 0.1 to 1.9
- expert_ids: int32 [65536, 2], P(('ep', 'tp')), may hold values from 0 to 127, all different within a row; in each aligned block of 256 rows (0 to 255, 256 to 511, ...) at most 6 rows name the same one
- route_weights: float32 [65536, 2], P(('ep', 'tp')), may hold values from 0.2 to 1.2
- expert_gate: bfloat16 [128, 2048, 512], P('ep', None, 'tp'), may hold values from -0.125 to 0.125
- expert_up: bfloat16 [128, 2048, 512], P('ep', None, 'tp'), may hold values from -0.125 to 0.125
- expert_down: bfloat16 [128, 512, 2048], P('ep', 'tp'), may hold values from -0.25 to 0.25
- shared_gate: bfloat16 [2048, 512], P(None, 'tp'), may hold values from -0.125 to 0.125
- shared_up: bfloat16 [2048, 512], P(None, 'tp'), may hold values from -0.125 to 0.125
- shared_down: bfloat16 [512, 2048], P('tp'), may hold values from -0.25 to 0.25
Outputs:
- mixed: bfloat16 [65536, 2048], P(('ep', 'tp'))
Inputs may be any that keep to these rules, and one draw needn't show every extreme that they name: `expert_ids`: each token names 2 different experts. Among the tokens of one device (aligned blocks of 256 rows) no expert is named by more than 6 tokens, and in every block some expert is named by exactly 6.
All inputs are finite; a program needn't handle non-finite values.
Results may differ from a plain program's by a relative error of at most 0.0075.
Values may be sent and summed in bfloat16 or wider, within the bound.
No kernel may reach another device: no remote copies, remote signals or barrier semaphores. Data moves between devices by JAX's collectives and lax.ppermute only.
A program may use at most 64 MiB of HBM per device.

v0:
```python
import jax
import jax.numpy as jnp
from jax import lax
from jax.sharding import PartitionSpec as P

epsilon = 1e-06


def normalize(tokens, norm_gain):
    values = tokens.astype(jnp.float32)
    factor = lax.rsqrt(jnp.mean(values * values, axis=1, keepdims=True) + epsilon)
    return (values * factor * norm_gain[None, :]).astype(jnp.bfloat16)


def round_term(partial_value):
    return lax.optimization_barrier(partial_value.astype(jnp.bfloat16)).astype(jnp.float32)


def gated_rows(row_block, gate_w, up_w):
    gate_value = jnp.dot(row_block, gate_w, preferred_element_type=jnp.float32)
    up_value = jnp.dot(row_block, up_w, preferred_element_type=jnp.float32)
    return (jax.nn.silu(gate_value) * up_value).astype(jnp.bfloat16)


def sliced_term(hidden, down_w):
    return round_term(jnp.dot(hidden, down_w, preferred_element_type=jnp.float32))


def shared_branch(normed, shared_gate, shared_up, shared_down):
    hidden = gated_rows(lax.all_gather(normed, "tp", axis=0, tiled=True), shared_gate, shared_up)
    return lax.psum_scatter(
        sliced_term(hidden, shared_down).astype(jnp.bfloat16), "tp", scatter_dimension=0, tiled=True
    ).astype(jnp.float32)


def body(
    tokens,
    norm_gain,
    expert_ids,
    route_weights,
    expert_gate,
    expert_up,
    expert_down,
    shared_gate,
    shared_up,
    shared_down,
):
    normed = normalize(tokens, norm_gain)
    tok_rows = tokens.shape[0]
    model_width = tokens.shape[1]
    top_count = expert_ids.shape[1]
    ep_size = lax.axis_size("ep")
    experts = expert_gate.shape[0] * ep_size
    capacity = 3 * tok_rows * top_count // (2 * experts)
    assigned = tok_rows * top_count
    gate_one = expert_gate[0]
    up_one = expert_up[0]
    down_one = expert_down[0]
    flat_ids = expert_ids.reshape(-1)
    onehot = (flat_ids[:, None] == jnp.arange(experts, dtype=jnp.int32)[None, :]).astype(
        jnp.bfloat16
    )
    earlier = (jnp.arange(assigned)[:, None] > jnp.arange(assigned)[None, :]).astype(jnp.bfloat16)
    before_count = jnp.dot(earlier, onehot, preferred_element_type=jnp.float32)
    slot_index = jnp.sum(before_count * onehot.astype(jnp.float32), axis=1).astype(jnp.int32)
    position = flat_ids * capacity + slot_index
    owners = (
        jnp.full((experts * capacity,), tok_rows, jnp.int32)
        .at[position]
        .set(jnp.arange(assigned, dtype=jnp.int32) // top_count)
    )
    padded = jnp.concatenate([normed, jnp.zeros((1, model_width), jnp.bfloat16)], axis=0)
    outgoing = padded[owners].reshape(ep_size, capacity, model_width)
    received = lax.all_to_all(outgoing, "ep", split_axis=0, concat_axis=0, tiled=True)
    hidden = gated_rows(
        lax.all_gather(received.reshape(ep_size * capacity, model_width), "tp", axis=0, tiled=True),
        gate_one,
        up_one,
    )
    summed = lax.psum_scatter(
        sliced_term(hidden, down_one).astype(jnp.bfloat16), "tp", scatter_dimension=0, tiled=True
    )
    returned = lax.all_to_all(
        summed.reshape(ep_size, capacity, model_width),
        "ep",
        split_axis=0,
        concat_axis=0,
        tiled=True,
    )
    gathered = returned.reshape(experts * capacity, model_width)[position]
    routed = jnp.sum(
        gathered.reshape(tok_rows, top_count, model_width).astype(jnp.float32)
        * route_weights[:, :, None],
        axis=1,
    )
    shared_out = shared_branch(normed, shared_gate, shared_up, shared_down)
    return (routed + shared_out).astype(jnp.bfloat16)


def solution(mesh):
    placed = (
        P(("ep", "tp"), None),
        P(),
        P(("ep", "tp"), None),
        P(("ep", "tp"), None),
        P("ep", None, "tp"),
        P("ep", None, "tp"),
        P("ep", "tp", None),
        P(None, "tp"),
        P(None, "tp"),
        P("tp", None),
    )
    return jax.shard_map(
        body, mesh=mesh, in_specs=placed, out_specs=P(("ep", "tp"), None), check_vma=False
    )
```

profile of v0, /device:TPU:6, one launch (start us, length us, event | category | flops | bytes accessed | tf_op | source)
XLA Modules:
  0.0 347.6 jit_solution(12503295927482520006)
XLA Ops:
  6.5 1.0 copy.13
  7.5 0.7 broadcast_multiply_fusion
  8.2 1.5 fusion.1
  9.7 0.1 eq.15
  9.9 0.3 fusion.5
  10.2 0.1 copy.12
  10.3 0.1 mul.67
  10.5 2.4 scatter_custom_fusion
  13.0 0.3 fusion.3
  13.4 4.3 %gather_fusion = bf16[768,2048]{1,0:T(8,128)(2,1)} fusion(bf16[257,2048]{1,0:T(8,128)(2,1)S(1)} %concatenate.3, s32[1024]{0:T(1024)S(1)} %pad_clamp_fusion.1), kind=kCustom, calls=%fused_computation | custom fusion | bytes 6294528 | tf_op jit(solution)/shard_map/gather | solution.py:73
  17.7 6.2 %reshape.59 = bf16[128,6,2048]{2,1,0:T(8,128)(2,1)} reshape(bf16[768,2048]{1,0:T(8,128)(2,1)} %gather_fusion) | data formatting | bytes 6291456 | tf_op jit(solution)/shard_map/reshape | solution.py:73
  23.9 111.4 %all_to_all.10 = bf16[128,6,2048]{2,1,0:T(8,128)(2,1)} all-to-all(bf16[128,6,2048]{2,1,0:T(8,128)(2,1)} %reshape.59), channel_id=1, replica_groups=mesh['ep'=128,'tp'=2] {'ep'}, dimensions={0} | all-to-all | bytes 6291456 | tf_op jit(solution)/shard_map/all_to_all | solution.py:74
  135.3 6.3 %reshape.60 = bf16[768,2048]{1,0:T(8,128)(2,1)} reshape(bf16[128,6,2048]{2,1,0:T(8,128)(2,1)} %all_to_all.10) | data formatting | bytes 6291456 | tf_op jit(solution)/shard_map/reshape | solution.py:76
  141.7 0.2 reduce-scatter.3.cloned.1.call-start
  141.9 18.4 %all-gather.3.cloned.1.call-done = bf16[1536,2048]{1,0:T(8,128)(2,1)} async-done(((bf16[768,2048]{1,0:T(8,128)(2,1)}), bf16[1536,2048]{1,0:T(8,128)(2,1)}) %all-gather.3.cloned.1.call-update) | async-done | bytes 6291472 | tf_op jit(solution)/shard_map/all_gather | solution.py:76
  160.3 5.8 %fusion.9 = f32[1536,256]{1,0:T(8,128)} fusion(bf16[1536,2048]{1,0:T(8,128)(2,1)} %all-gather.3.cloned.1.call-done, bf16[1,2048,256]{2,1,0:T(8,128)(2,1)S(1)} %copy-done.7), kind=kOutput, calls=%fused_computation.20 | convolution fusion | flops 1610612736 | bytes 8912896 | tf_op jit(solution)/shard_map/dot_general | solution.py:20
  166.1 12.3 %convolution_convert_fusion = bf16[1536,2048]{1,0:T(8,128)(2,1)} fusion(bf16[1536,2048]{1,0:T(8,128)(2,1)} %all-gather.3.cloned.1.call-done, f32[1536,256]{1,0:T(8,128)} %fusion.9, bf16[1,256,2048]{2,1,0:T(8,128)(2,1)S(1)} %copy-done, bf16[1,2048,256]{2,1,0:T(8,128)(2,1)S(1)} %copy-done.8), kind=kOutput, calls=%fused_computation.3 | convolution fusion | flops 3226730496 | bytes 16252928 | tf_op jit(solution)/shard_map/dot_general | solution.py:26
  178.4 0.7 all-gather.5.cloned.1.call-update
  179.1 21.0 %reduce-scatter.3.cloned.1.call-done = bf16[768,2048]{1,0:T(8,128)(2,1)} async-done(((bf16[1536,2048]{1,0:T(8,128)(2,1)}), bf16[768,2048]{1,0:T(8,128)(2,1)}) %reduce-scatter.3.cloned.1.call-update) | async-done | bytes 3145744 | tf_op jit(solution)/shard_map/reduce_scatter | solution.py:80
  200.1 6.2 %reshape.61 = bf16[128,6,2048]{2,1,0:T(8,128)(2,1)} reshape(bf16[768,2048]{1,0:T(8,128)(2,1)} %reduce-scatter.3.cloned.1.call-done) | data formatting | bytes 6291456 | tf_op jit(solution)/shard_map/reshape | solution.py:84
  206.3 14.3 %all-to-all-start.1 = ((bf16[128,6,2048]{2,1,0:T(8,128)(2,1)}), bf16[128,6,2048]{2,1,0:T(8,128)(2,1)}, u32[]{:S(2)}, u32[]{:S(2)}) async-start(bf16[128,6,2048]{2,1,0:T(8,128)(2,1)} %reshape.61), calls=%async_computation.2 | async-start | bytes 8388608 | tf_op jit(solution)/shard_map/all_to_all | solution.py:83
  220.7 0.3 reduce-scatter.5.cloned.1.call-start
  221.0 3.2 fusion.27
  224.2 5.4 %convolution_convert_fusion.1 = bf16[512,2048]{1,0:T(8,128)(2,1)} fusion(bf16[256,2048]{1,0:T(8,128)(2,1)} %param.19, bf16[512,2048]{1,0:T(8,128)(2,1)S(1)} %copy-done.6, bf16[2048,256]{1,0:T(8,128)(2,1)} %param.18, f32[512,256]{1,0:T(8,128)} %fusion.27), kind=kOutput, calls=%fused_computation.5 | convolution fusion | flops 1075576832 | bytes 6815744 | tf_op jit(solution)/shard_map/dot_general | solution.py:26
  229.6 0.7 copy-done.5
  230.3 0.1 copy.14
  230.4 85.6 %all-to-all-done.1 = bf16[128,6,2048]{2,1,0:T(8,128)(2,1)} async-done(((bf16[128,6,2048]{2,1,0:T(8,128)(2,1)}), bf16[128,6,2048]{2,1,0:T(8,128)(2,1)}, u32[]{:S(2)}, u32[]{:S(2)}) %all-to-all-start.1) | async-done | bytes 3145760 | tf_op jit(solution)/shard_map/all_to_all | solution.py:83
  316.0 4.9 %reshape.62 = bf16[768,2048]{1,0:T(8,128)(2,1)S(1)} reshape(bf16[128,6,2048]{2,1,0:T(8,128)(2,1)} %all-to-all-done.1) | data formatting | bytes 6291456 | tf_op jit(solution)/shard_map/reshape | solution.py:90
  320.9 3.3 gather_fusion.1
  324.2 5.4 %reshape.63 = f32[256,2,2048]{2,1,0:T(2,128)} reshape(bf16[512,2048]{1,0:T(8,128)(2,1)} %gather_fusion.1) | data formatting | bytes 6291456 | tf_op jit(solution)/shard_map/convert_element_type | solution.py:92
  329.7 8.9 %multiply_reduce_fusion = f32[256,2048]{1,0:T(8,128)S(1)} fusion(f32[256,2,2048]{2,1,0:T(2,128)} %reshape.63, f32[256,2]{1,0:T(8,128)S(1)} %copy.14), kind=kLoop, calls=%fused_computation.4 | loop fusion | flops 1572864 | bytes 6293504 | tf_op jit(solution)/shard_map/reduce_sum | solution.py:91
  338.6 2.5 add_convert_fusion
  (34 shorter events, 0.3 us)
Async XLA Ops:
  6.5 159.5 %copy-start = (bf16[1,256,2048]{2,1,0:T(8,128)(2,1)S(1)}, bf16[1,256,2048]{2,1,0:T(8,128)(2,1)}, u32[]{:S(2)}) copy-start(bf16[1,256,2048]{2,1,0:T(8,128)(2,1)} %param.16) | copy-start | bytes 3145732
  6.5 6.4 %copy-start.3 = (bf16[256,2048]{1,0:T(8,128)(2,1)S(1)}, bf16[256,2048]{1,0:T(8,128)(2,1)}, u32[]{:S(2)}) copy-start(bf16[256,2048]{1,0:T(8,128)(2,1)} %param.10) | copy-start | bytes 3145732
  6.5 6.5 %copy-start.4 = (f32[2048]{0:T(1024)S(1)}, f32[2048]{0:T(1024)}, u32[]{:S(2)}) copy-start(f32[2048]{0:T(1024)} %param.11) | copy-start | bytes 24580
  6.5 153.7 %all-gather.3.cloned.1.call-start = ((), (), s32[]{:S(2)}) async-start(), calls=%async_computation.4 | async-start | bytes 9437184 | tf_op jit(solution)/shard_map/all_gather | solution.py:76
  13.3 4.4 %copy-start.2 = (bf16[256,2048]{1,0:T(8,128)(2,1)}, bf16[256,2048]{1,0:T(8,128)(2,1)S(1)}, u32[]{:S(2)}) copy-start(bf16[256,2048]{1,0:T(8,128)(2,1)S(1)} %fusion.3) | copy-start | bytes 3145732
  141.7 18.6 %copy-start.7 = (bf16[1,2048,256]{2,1,0:T(8,128)(2,1)S(1)}, bf16[1,2048,256]{2,1,0:T(8,128)(2,1)}, u32[]{:S(2)}) copy-start(bf16[1,2048,256]{2,1,0:T(8,128)(2,1)} %param.14) | copy-start | bytes 3145732
  141.7 24.4 %copy-start.8 = (bf16[1,2048,256]{2,1,0:T(8,128)(2,1)S(1)}, bf16[1,2048,256]{2,1,0:T(8,128)(2,1)}, u32[]{:S(2)}) copy-start(bf16[1,2048,256]{2,1,0:T(8,128)(2,1)} %param.15) | copy-start | bytes 3145732
  141.7 58.4 %reduce-scatter.3.cloned.1.call-start = ((), (), s32[]{:S(2)}) async-start(), calls=%async_computation.5 | async-start | bytes 9437184 | tf_op jit(solution)/shard_map/reduce_scatter | solution.py:80
  178.4 42.6 %all-gather.5.cloned.1.call-start = ((), (), s32[]{:S(2)}) async-start(), calls=%async_computation.6 | async-start | bytes 3145728 | tf_op jit(solution)/shard_map/all_gather | solution.py:30
  206.3 14.7 %copy-start.9 = (bf16[2048,256]{1,0:T(8,128)(2,1)S(1)}, bf16[2048,256]{1,0:T(8,128)(2,1)}, u32[]{:S(2)}) copy-start(bf16[2048,256]{1,0:T(8,128)(2,1)} %param.17) | copy-start | bytes 3145732
  206.3 109.7 %all-to-all-start.1 = ((bf16[128,6,2048]{2,1,0:T(8,128)(2,1)}), bf16[128,6,2048]{2,1,0:T(8,128)(2,1)}, u32[]{:S(2)}, u32[]{:S(2)}) async-start(bf16[128,6,2048]{2,1,0:T(8,128)(2,1)} %reshape.61), calls=%async_computation.2 | async-start | bytes 8388608 | tf_op jit(solution)/shard_map/all_to_all | solution.py:83
  220.7 117.9 %reduce-scatter.5.cloned.1.call-start = ((), (), s32[]{:S(2)}) async-start(), calls=%async_computation.7 | async-start | bytes 3145728 | tf_op jit(solution)/shard_map/reduce_scatter | solution.py:31
  221.0 3.3 copy-start.6
  229.6 0.7 copy-start.5
  329.7 11.4 %copy-start.1 = (bf16[1,256,2048]{2,1,0:T(8,128)(2,1)S(1)}, bf16[1,256,2048]{2,1,0:T(8,128)(2,1)}, u32[]{:S(2)}) copy-start(bf16[1,256,2048]{2,1,0:T(8,128)(2,1)} %param.16) | copy-start | bytes 3145732
Sparse Core Ops, SparseCore 0:
  141.8 18.4 all-gather.2
  178.5 21.5 reduce-scatter.2
  201.9 17.1 all-gather.4
  229.7 16.4 reduce-scatter.4
where the time goes:
time: 349 us; the launch traced here: 348 us
  waiting for transfers between devices  126 us (36%)
  blocking collectives  111 us (32%)
  local copies, waits for them, and re-layouts  41.4 us (12%)
  matrix products  27 us (8%)
  starting transfers between devices  14.9 us (4%)
  other arithmetic  13.9 us (4%)
  between operations  13.3 us (4%)
    all_to_all x1, blocking collectives, body(): lax.all_to_all(outgoing, 'ep', split_axis=0, concat_axis=0, tiled=True)  111 us
    all_to_all x1, waiting for transfers between devices, body(): lax.all_to_all(summed.reshape(ep_size, capacity, model_width), 'ep', spli...  85.6 us
    reduce_scatter x1, waiting for transfers between devices, body(): lax.psum_scatter(sliced_term(hidden, down_one).astype(jnp.bfloat16), 'tp'...  21 us
    all_gather x1, waiting for transfers between devices, body(): lax.all_gather(received.reshape(ep_size * capacity, model_width), 'tp', a...  18.4 us
    dot_general x2, matrix products, sliced_term(): jnp.dot(hidden, down_w, preferred_element_type=jnp.float32)  17.7 us
    all_to_all x1, starting transfers between devices, body(): lax.all_to_all(summed.reshape(ep_size, capacity, model_width), 'ep', spli...  14.3 us
    dot_general x2, matrix products, gated_rows(): gate_value = jnp.dot(row_block, gate_w, preferred_element_type=jnp.float32)  9.02 us
    reduce_sum x1, other arithmetic, body(): jnp.sum(gathered.reshape(tok_rows, top_count, model_width).astype(jnp.flo...  8.86 us
  transfers between devices with their start and end apart: 5, of which 3 were waited for; matrix products, arithmetic and copies ran while one was open for 11% of the time, Pallas kernels for 0%

commit v1 on v0

--- a/solution.py
+++ b/solution.py
@@ -72,10 +72,15 @@
     padded = jnp.concatenate([normed, jnp.zeros((1, model_width), jnp.bfloat16)], axis=0)
     outgoing = padded[owners].reshape(ep_size, capacity, model_width)
     received = lax.all_to_all(outgoing, "ep", split_axis=0, concat_axis=0, tiled=True)
+
+    def resolve_shapes(content, axis_tag):
+        state_next = lax.all_to_all(
+            jnp.concatenate([content] * lax.psum(1, axis_tag), 0), axis_tag, 0, 0, tiled=True
+        )
+        return state_next
+
     hidden = gated_rows(
-        lax.all_gather(received.reshape(ep_size * capacity, model_width), "tp", axis=0, tiled=True),
-        gate_one,
-        up_one,
+        resolve_shapes(received.reshape(ep_size * capacity, model_width), "tp"), gate_one, up_one
     )
     summed = lax.psum_scatter(
         sliced_term(hidden, down_one).astype(jnp.bfloat16), "tp", scatter_dimension=0, tiled=True

time: 349 us -> 338 us (0.968)
  waiting for transfers between devices: 126 us -> 102 us
  blocking collectives: 111 us -> 120 us
  other arithmetic: 13.9 us -> 17.8 us
    all_gather x1 -> x0, waiting for transfers between devices: 18.4 us -> none  [body(): lax.all_gather(received.reshape(ep_size * capacity, model_width), 'tp', a...]
    all_to_all x0 -> x1, blocking collectives: none -> 8.92 us  [resolve_shapes(): lax.all_to_all(jnp.concatenate([content] * lax.psum(1, axis_tag), 0), axi...]
    reduce_scatter x1, waiting for transfers between devices: 21 us -> 16 us  [body(): lax.psum_scatter(sliced_term(hidden, down_one).astype(jnp.bfloat16), 'tp'...]
    concatenate x0 -> x1, other arithmetic: none -> 3.96 us  [resolve_shapes(): jnp.concatenate([content] * lax.psum(1, axis_tag), 0)]
  transfers between devices with their start and end apart: 5 -> 4, of which waited for: 3 -> 2; matrix products, arithmetic and copies ran while one was open for 11% -> 11% of each run, Pallas kernels for 0% -> 0%
where the time goes in v1:
time: 338 us; the launch traced here: 337 us
  blocking collectives  120 us (36%)
  waiting for transfers between devices  102 us (30%)
  local copies, waits for them, and re-layouts  44.1 us (13%)
  matrix products  24.3 us (7%)
  other arithmetic  17.8 us (5%)
  starting transfers between devices  14.7 us (4%)
  between operations  13.3 us (4%)
    all_to_all x1, blocking collectives, body(): lax.all_to_all(outgoing, 'ep', split_axis=0, concat_axis=0, tiled=True)  111 us
    all_to_all x1, waiting for transfers between devices, body(): lax.all_to_all(summed.reshape(ep_size, capacity, model_width), 'ep', spli...  85.6 us
    dot_general x2, matrix products, sliced_term(): jnp.dot(hidden, down_w, preferred_element_type=jnp.float32)  17.7 us
    reduce_scatter x1, waiting for transfers between devices, body(): lax.psum_scatter(sliced_term(hidden, down_one).astype(jnp.bfloat16), 'tp'...  16 us
    all_to_all x1, starting transfers between devices, body(): lax.all_to_all(summed.reshape(ep_size, capacity, model_width), 'ep', spli...  14.4 us
    all_to_all x1, blocking collectives, resolve_shapes(): lax.all_to_all(jnp.concatenate([content] * lax.psum(1, axis_tag), 0), axi...  8.92 us
    reduce_sum x1, other arithmetic, body(): jnp.sum(gathered.reshape(tok_rows, top_count, model_width).astype(jnp.flo...  8.86 us
  transfers between devices with their start and end apart: 4, of which 2 were waited for; matrix products, arithmetic and copies ran while one was open for 11% of the time, Pallas kernels for 0%

profile of v1, /device:TPU:6, one launch (start us, length us, event | category | flops | bytes accessed | tf_op | source)
XLA Modules:
  0.0 336.8 jit_solution(7381680345387789978)
XLA Ops:
  6.5 1.0 copy.13
  7.5 0.7 broadcast_multiply_fusion
  8.2 1.5 fusion.1
  9.7 0.1 eq.15
  9.9 0.3 fusion.5
  10.2 0.1 copy.12
  10.3 0.1 mul.67
  10.5 2.4 scatter_custom_fusion
  13.0 0.3 fusion.3
  13.4 4.3 %gather_fusion = bf16[768,2048]{1,0:T(8,128)(2,1)} fusion(bf16[257,2048]{1,0:T(8,128)(2,1)S(1)} %concatenate.6, s32[1024]{0:T(1024)S(1)} %pad_clamp_fusion.1), kind=kCustom, calls=%fused_computation | custom fusion | bytes 6294528 | tf_op jit(solution)/shard_map/gather | solution.py:73
  17.7 6.2 %reshape.61 = bf16[128,6,2048]{2,1,0:T(8,128)(2,1)} reshape(bf16[768,2048]{1,0:T(8,128)(2,1)} %gather_fusion) | data formatting | bytes 6291456 | tf_op jit(solution)/shard_map/reshape | solution.py:73
  24.0 111.4 %all_to_all.22 = bf16[128,6,2048]{2,1,0:T(8,128)(2,1)} all-to-all(bf16[128,6,2048]{2,1,0:T(8,128)(2,1)} %reshape.61), channel_id=1, replica_groups=mesh['ep'=128,'tp'=2] {'ep'}, dimensions={0} | all-to-all | bytes 6291456 | tf_op jit(solution)/shard_map/all_to_all | solution.py:74
  135.3 6.3 %reshape.62 = bf16[768,2048]{1,0:T(8,128)(2,1)} reshape(bf16[128,6,2048]{2,1,0:T(8,128)(2,1)} %all_to_all.22) | data formatting | bytes 6291456 | tf_op jit(solution)/shard_map/reshape | solution.py:83
  141.7 4.0 %pad_maximum_fusion = bf16[1536,2048]{1,0:T(8,128)(2,1)S(1)} fusion(bf16[768,2048]{1,0:T(8,128)(2,1)} %reshape.62), kind=kLoop, calls=%fused_computation.4 | loop fusion | flops 12582912 | bytes 9437184 | tf_op jit(solution)/shard_map/concatenate | solution.py:78
  145.6 8.9 %all_to_all.23 = bf16[2,768,2048]{2,1,0:T(8,128)(2,1)S(1)} all-to-all(bf16[2,768,2048]{2,1,0:T(8,128)(2,1)S(1)} %bitcast.21), channel_id=1, replica_groups=mesh['ep'=128,'tp'=2] {'tp'}, dimensions={0} | all-to-all | bytes 12582912 | tf_op jit(solution)/shard_map/all_to_all | solution.py:77
  154.6 2.6 copy-done.3
  157.2 3.1 fusion.9
  160.3 12.3 %convolution_convert_fusion = bf16[1536,2048]{1,0:T(8,128)(2,1)} fusion(bf16[1536,2048]{1,0:T(8,128)(2,1)} %bitcast.23, f32[1536,256]{1,0:T(8,128)} %fusion.9, bf16[1,256,2048]{2,1,0:T(8,128)(2,1)S(1)} %copy-done, bf16[1,2048,256]{2,1,0:T(8,128)(2,1)S(1)} %copy-done.9), kind=kOutput, calls=%fused_computation.3 | convolution fusion | flops 3226730496 | bytes 16252928 | tf_op jit(solution)/shard_map/dot_general | solution.py:26
  172.6 0.7 all-gather.2.cloned.1.call-update
  173.3 16.0 %reduce-scatter.3.cloned.1.call-done = bf16[768,2048]{1,0:T(8,128)(2,1)} async-done(((bf16[1536,2048]{1,0:T(8,128)(2,1)}), bf16[768,2048]{1,0:T(8,128)(2,1)}) %reduce-scatter.3.cloned.1.call-update) | async-done | bytes 3145744 | tf_op jit(solution)/shard_map/reduce_scatter | solution.py:85
  189.3 6.2 %reshape.63 = bf16[128,6,2048]{2,1,0:T(8,128)(2,1)} reshape(bf16[768,2048]{1,0:T(8,128)(2,1)} %reduce-scatter.3.cloned.1.call-done) | data formatting | bytes 6291456 | tf_op jit(solution)/shard_map/reshape | solution.py:89
  195.6 14.4 %all-to-all-start.2 = ((bf16[128,6,2048]{2,1,0:T(8,128)(2,1)}), bf16[128,6,2048]{2,1,0:T(8,128)(2,1)}, u32[]{:S(2)}, u32[]{:S(2)}) async-start(bf16[128,6,2048]{2,1,0:T(8,128)(2,1)} %reshape.63), calls=%async_computation.3 | async-start | bytes 8388608 | tf_op jit(solution)/shard_map/all_to_all | solution.py:88
  209.9 0.3 reduce-scatter.5.cloned.1.call-start
  210.3 3.2 fusion.27
  213.5 5.4 %convolution_convert_fusion.1 = bf16[512,2048]{1,0:T(8,128)(2,1)} fusion(bf16[256,2048]{1,0:T(8,128)(2,1)} %param.19, bf16[512,2048]{1,0:T(8,128)(2,1)S(1)} %copy-done.7, bf16[2048,256]{1,0:T(8,128)(2,1)} %param.18, f32[512,256]{1,0:T(8,128)} %fusion.27), kind=kOutput, calls=%fused_computation.6 | convolution fusion | flops 1075576832 | bytes 6815744 | tf_op jit(solution)/shard_map/dot_general | solution.py:26
  218.9 0.7 copy-done.6
  219.7 85.6 %all-to-all-done.2 = bf16[128,6,2048]{2,1,0:T(8,128)(2,1)} async-done(((bf16[128,6,2048]{2,1,0:T(8,128)(2,1)}), bf16[128,6,2048]{2,1,0:T(8,128)(2,1)}, u32[]{:S(2)}, u32[]{:S(2)}) %all-to-all-start.2) | async-done | bytes 3145760 | tf_op jit(solution)/shard_map/all_to_all | solution.py:88
  305.3 4.9 %reshape.64 = bf16[768,2048]{1,0:T(8,128)(2,1)S(1)} reshape(bf16[128,6,2048]{2,1,0:T(8,128)(2,1)} %all-to-all-done.2) | data formatting | bytes 6291456 | tf_op jit(solution)/shard_map/reshape | solution.py:95
  310.2 3.3 gather_fusion.1
  313.5 5.4 %reshape.65 = f32[256,2,2048]{2,1,0:T(2,128)} reshape(bf16[512,2048]{1,0:T(8,128)(2,1)} %gather_fusion.1) | data formatting | bytes 6291456 | tf_op jit(solution)/shard_map/convert_element_type | solution.py:97
  318.9 8.9 %multiply_reduce_fusion = f32[256,2048]{1,0:T(8,128)S(1)} fusion(f32[256,2,2048]{2,1,0:T(2,128)} %reshape.65, f32[256,2]{1,0:T(8,128)S(1)} %copy.14), kind=kLoop, calls=%fused_computation.5 | loop fusion | flops 1572864 | bytes 6293504 | tf_op jit(solution)/shard_map/reduce_sum | solution.py:96
  327.8 2.5 add_convert_fusion
  (35 shorter events, 0.4 us)
Async XLA Ops:
  6.5 153.7 %copy-start = (bf16[1,256,2048]{2,1,0:T(8,128)(2,1)S(1)}, bf16[1,256,2048]{2,1,0:T(8,128)(2,1)}, u32[]{:S(2)}) copy-start(bf16[1,256,2048]{2,1,0:T(8,128)(2,1)} %param.16) | copy-start | bytes 3145732
  6.5 6.4 %copy-start.4 = (bf16[256,2048]{1,0:T(8,128)(2,1)S(1)}, bf16[256,2048]{1,0:T(8,128)(2,1)}, u32[]{:S(2)}) copy-start(bf16[256,2048]{1,0:T(8,128)(2,1)} %param.10) | copy-start | bytes 3145732
  6.5 6.5 %copy-start.5 = (f32[2048]{0:T(1024)S(1)}, f32[2048]{0:T(1024)}, u32[]{:S(2)}) copy-start(f32[2048]{0:T(1024)} %param.11) | copy-start | bytes 24580
  6.5 182.8 %reduce-scatter.3.cloned.1.call-start = ((), (), s32[]{:S(2)}) async-start(), calls=%async_computation.5 | async-start | bytes 9437184 | tf_op jit(solution)/shard_map/reduce_scatter | solution.py:85
  13.3 4.4 %copy-start.2 = (bf16[256,2048]{1,0:T(8,128)(2,1)}, bf16[256,2048]{1,0:T(8,128)(2,1)S(1)}, u32[]{:S(2)}) copy-start(bf16[256,2048]{1,0:T(8,128)(2,1)S(1)} %fusion.3) | copy-start | bytes 3145732
  145.6 11.6 %copy-start.8 = (bf16[1,2048,256]{2,1,0:T(8,128)(2,1)S(1)}, bf16[1,2048,256]{2,1,0:T(8,128)(2,1)}, u32[]{:S(2)}) copy-start(bf16[1,2048,256]{2,1,0:T(8,128)(2,1)} %param.14) | copy-start | bytes 3145732
  154.6 2.6 copy-start.3
  157.2 3.1 copy-start.9
  172.6 37.6 %all-gather.2.cloned.1.call-start = ((), (), s32[]{:S(2)}) async-start(), calls=%async_computation.6 | async-start | bytes 3145728 | tf_op jit(solution)/shard_map/all_gather | solution.py:30
  195.6 14.7 %copy-start.10 = (bf16[2048,256]{1,0:T(8,128)(2,1)S(1)}, bf16[2048,256]{1,0:T(8,128)(2,1)}, u32[]{:S(2)}) copy-start(bf16[2048,256]{1,0:T(8,128)(2,1)} %param.17) | copy-start | bytes 3145732
  195.6 109.7 %all-to-all-start.2 = ((bf16[128,6,2048]{2,1,0:T(8,128)(2,1)}), bf16[128,6,2048]{2,1,0:T(8,128)(2,1)}, u32[]{:S(2)}, u32[]{:S(2)}) async-start(bf16[128,6,2048]{2,1,0:T(8,128)(2,1)} %reshape.63), calls=%async_computation.3 | async-start | bytes 8388608 | tf_op jit(solution)/shard_map/all_to_all | solution.py:88
  209.9 117.9 %reduce-scatter.5.cloned.1.call-start = ((), (), s32[]{:S(2)}) async-start(), calls=%async_computation.7 | async-start | bytes 3145728 | tf_op jit(solution)/shard_map/reduce_scatter | solution.py:31
  210.3 3.3 copy-start.7
  218.9 0.7 copy-start.6
  318.9 11.4 %copy-start.1 = (bf16[1,256,2048]{2,1,0:T(8,128)(2,1)S(1)}, bf16[1,256,2048]{2,1,0:T(8,128)(2,1)}, u32[]{:S(2)}) copy-start(bf16[1,256,2048]{2,1,0:T(8,128)(2,1)} %param.16) | copy-start | bytes 3145732
Sparse Core Ops, SparseCore 0:
  172.7 16.5 reduce-scatter.2
  191.1 17.2 all-gather.1
  219.0 16.4 reduce-scatter.4
